TPU v7x, 256 devices: a whole 4x4x8 slice. The times are simulated.
256 devices in a mesh: dp: 4 (over y), kv: 32 (over z, x), tp: 2 (over core).
Axes of the slice: x: 4, y: 4, z: 8, core: 2. Of those that a mesh axis runs over, the one named last changes fastest.
Arguments:
- tokens: bfloat16 [2048, 2048], P('dp', ('kv', 'tp')), parts along dimension 0, may hold values from -64 to 64, as said below
- lengths: int32 [256], P(('dp', 'kv', 'tp')), parts along dimension 0, may hold values from 1 to 8, 224 in all
- state: float32 [256, 16, 128, 128], P(('dp', 'kv', 'tp')), parts along dimension 0, may hold values from -1.8 to 1.8
- gain_first: float32 [2048], replicated, may hold values from 0.1 to 1.9
- first_gate: bfloat16 [2048, 5632], P(None, 'kv'), may hold values from -0.125 to 0.125
- first_up: bfloat16 [2048, 5632], P(None, 'kv'), may hold values from -0.125 to 0.125
- first_down: bfloat16 [5632, 2048], P('kv'), may hold values from -0.15625 to 0.15625
- gain_mix: float32 [2048], replicated, may hold values from 0.1 to 1.9
- query_weight: bfloat16 [2048, 2048], P(None, ('kv', 'tp')), may hold values from -0.125 to 0.125
- key_weight: bfloat16 [2048, 2048], P(None, ('kv', 'tp')), may hold values from -0.125 to 0.125
- value_weight: bfloat16 [2048, 2048], P(None, ('kv', 'tp')), may hold values from -0.125 to 0.125
- gating_weight: bfloat16 [2048, 2048], P(None, ('kv', 'tp')), may hold values from -0.125 to 0.125
- write_weight: bfloat16 [2048, 16], replicated, may hold values from -0.125 to 0.125
- forget_weight: bfloat16 [2048, 16], replicated, may hold values from -0.125 to 0.125
- forget_rate: float32 [16], replicated, may hold values from -4 to 1.5
- out_weight: bfloat16 [2048, 2048], P(None, ('kv', 'tp')), may hold values from -0.125 to 0.125
- gain_second: float32 [2048], replicated, may hold values from 0.1 to 1.9
- second_gate: bfloat16 [2048, 5632], P(None, 'kv'), may hold values from -0.125 to 0.125
- second_up: bfloat16 [2048, 5632], P(None, 'kv'), may hold values from -0.125 to 0.125
- second_down: bfloat16 [5632, 2048], P('kv'), may hold values from -0.15625 to 0.15625
Outputs:
- mixed_out: bfloat16 [2048, 2048], P('dp', ('kv', 'tp')), parts along dimension 0
- new_state: float32 [256, 16, 128, 128], P(('dp', 'kv', 'tp')), parts along dimension 0
There are 4 independent parts, one for each index of `dp`. A program takes and returns all parts, laid end to end along the dimension named above; an argument that names none is the same for every part. Nothing has to cross between parts.
Inputs may be any that keep to these rules, and one draw needn't show every extreme that they name: Activations of the new tokens. `lengths`: the live new tokens of each sequence; within each independent group of 64 sequences (one part along dp) they sum to seven halves of 64, rounded down, and some sequence of each group has all 8 live.
All inputs are finite; a program needn't handle non-finite values.
Results may differ from a plain program's by a relative error of at most 0.0058.
Values may be sent and summed in bfloat16 or wider, within the bound.
A program may use at most 64 MiB of HBM per device.

v0:
```python
import math
import jax
import jax.numpy as jnp
from jax import lax
from jax.sharding import PartitionSpec as P

HEADS = 16
HEAD = 128
BLK = 8
EPSILON = 1e-06


def laid_out(parts, dim):
    parts = jnp.moveaxis(parts, 0, dim)
    dims = parts.shape
    return parts.reshape(*dims[:dim], dims[dim] * dims[dim + 1], *dims[dim + 2 :])


def copy_for_each(array, axis):
    copies = jnp.broadcast_to(array, (lax.axis_size(axis), *array.shape))
    return lax.all_to_all(copies, axis, split_axis=0, concat_axis=0, tiled=True)


def collect(array, axis, dim):
    return laid_out(copy_for_each(array, axis), dim)


def cut_along(array, dim, count):
    before, after = (array.shape[:dim], array.shape[dim + 1 :])
    return jnp.moveaxis(array.reshape(*before, count, -1, *after), dim, 0)


def sum_at_owner(array, axis, dim):
    parts = cut_along(array, dim, lax.axis_size(axis))
    arrived = lax.all_to_all(parts, axis, split_axis=0, concat_axis=0, tiled=True)
    return arrived.astype(jnp.float32).sum(axis=0)


def fold_step(gain, gate_cols, up_cols, portion):
    values = portion.astype(jnp.float32)
    scaled = (values * gain).astype(jnp.bfloat16)
    gate_acc = jnp.dot(scaled, gate_cols, preferred_element_type=jnp.float32)
    up_acc = jnp.dot(scaled, up_cols, preferred_element_type=jnp.float32)
    squares = jnp.sum(values * values, axis=1)
    return (gate_acc, up_acc, squares)


def finish_units(gate_acc, up_acc, squares, channels, down_rows):
    row_scale = lax.rsqrt(squares / channels + EPSILON)[:, None]
    hidden = (jax.nn.silu(gate_acc * row_scale) * (up_acc * row_scale)).astype(jnp.bfloat16)
    return jnp.dot(hidden, down_rows, preferred_element_type=jnp.float32)


def feed_forward(hidden_in, gain, w_gate, w_up, w_down):
    channels = gain.shape[0]
    paired = lax.all_to_all(hidden_in, "tp", split_axis=0, concat_axis=1, tiled=True)
    gate_acc, up_acc, squares = fold_step(gain, w_gate, w_up, collect(paired, "kv", 1))
    ffn_term = finish_units(gate_acc, up_acc, squares, channels, w_down)
    partial_value = sum_at_owner(ffn_term.astype(jnp.bfloat16), "kv", 1)
    summed = lax.all_to_all(partial_value, "tp", split_axis=1, concat_axis=0, tiled=True)
    return (hidden_in.astype(jnp.float32) + 0.5 * summed).astype(jnp.bfloat16)


def delta_block(query, key_in, value, gating, write_pre, forget_pre, rates, live, state):
    seq_count, block_len, head_count, head_size = query.shape
    precise = lax.Precision.HIGHEST
    query_unit = (
        query
        * lax.rsqrt(jnp.sum(query * query, axis=-1, keepdims=True) + EPSILON)
        / math.sqrt(head_size)
    )
    key_unit = key_in * lax.rsqrt(jnp.sum(key_in * key_in, axis=-1, keepdims=True) + EPSILON)
    live_rows = live[:, :, None]
    write_gate = jax.nn.sigmoid(write_pre) * live_rows
    forget = -jnp.exp(rates)[None, None, :] * jax.nn.softplus(forget_pre) * live_rows
    cumulative = jnp.cumsum(forget, axis=1)
    cum_heads = jnp.transpose(cumulative, (0, 2, 1))
    positions = jnp.arange(block_len)
    causal = positions[:, None] >= positions[None, :]
    strict = positions[:, None] > positions[None, :]
    differ = jnp.minimum(cum_heads[:, :, :, None] - cum_heads[:, :, None, :], 0.0)
    decay_mat = jnp.where(causal, jnp.exp(differ), 0.0)
    key_dots = jnp.einsum("sthd,suhd->shtu", key_unit, key_unit, precision=precise)
    write_heads = jnp.transpose(write_gate, (0, 2, 1))
    strict_part = jnp.where(strict, write_heads[:, :, :, None] * decay_mat * key_dots, 0.0)
    identity = jnp.eye(block_len, dtype=jnp.float32)
    squared = jnp.einsum("shtu,shuv->shtv", strict_part, strict_part, precision=precise)
    fourth = jnp.einsum("shtu,shuv->shtv", squared, squared, precision=precise)
    inverse = jnp.einsum(
        "shtu,shuv->shtv", identity - strict_part, identity + squared, precision=precise
    )
    inverse = jnp.einsum("shtu,shuv->shtv", inverse, identity + fourth, precision=precise)
    growth = jnp.exp(cumulative)
    target = jnp.einsum(
        "shtu,suhv->sthv", inverse, write_gate[..., None] * value, precision=precise
    )
    key_mix = jnp.einsum(
        "shtu,suhk->sthk", inverse, (write_gate * growth)[..., None] * key_unit, precision=precise
    )
    update = target - jnp.einsum("sthk,shkv->sthv", key_mix, state, precision=precise)
    scores = jnp.einsum("sthd,suhd->shtu", query_unit, key_unit, precision=precise) * decay_mat
    attend = jnp.einsum("sthk,shkv->sthv", query_unit * growth[..., None], state, precision=precise)
    attend = attend + jnp.einsum("shtu,suhv->sthv", scores, update, precision=precise)
    final_cum = cumulative[:, -1:, :]
    fading = jnp.exp(final_cum - cumulative)
    new_state = jnp.exp(final_cum[:, 0, :])[:, :, None, None] * state
    new_state = new_state + jnp.einsum(
        "sthk,sthv->shkv", key_unit * fading[..., None], update, precision=precise
    )
    normed = attend * lax.rsqrt(jnp.mean(attend * attend, axis=-1, keepdims=True) + EPSILON)
    normed = normed * jax.nn.silu(gating) * live[:, :, None, None]
    mixed_heads = normed.reshape(seq_count * block_len, head_count * head_size).astype(jnp.bfloat16)
    return (mixed_heads, new_state)


def per_device(
    tokens,
    lengths,
    state,
    gain_first,
    first_gate,
    first_up,
    first_down,
    gain_mix,
    query_weight,
    key_weight,
    value_weight,
    gating_weight,
    write_weight,
    forget_weight,
    forget_rate,
    out_weight,
    gain_second,
    second_gate,
    second_up,
    second_down,
):
    after_first = feed_forward(tokens, gain_first, first_gate, first_up, first_down)
    seq_count = lengths.shape[0]
    own_count = seq_count * BLK
    whole_rows = collect(after_first, ("kv", "tp"), 1)
    scaled_all = (whole_rows.astype(jnp.float32) * gain_mix).astype(jnp.bfloat16)
    stacked = jnp.stack(
        [
            jnp.dot(scaled_all, matrix, preferred_element_type=jnp.float32)
            for matrix in (query_weight, key_weight, value_weight, gating_weight)
        ]
    )
    owned = lax.all_to_all(
        stacked.astype(jnp.bfloat16), ("kv", "tp"), split_axis=1, concat_axis=2, tiled=True
    ).astype(stacked.dtype)
    row_start = lax.axis_index(("kv", "tp")) * own_count
    own_values = lax.dynamic_slice_in_dim(whole_rows, row_start, own_count, 0).astype(jnp.float32)
    own_scaled = lax.dynamic_slice_in_dim(scaled_all, row_start, own_count, 0)
    mix_scale = lax.rsqrt(jnp.mean(own_values * own_values, axis=1, keepdims=True) + EPSILON)
    query = (owned[0] * mix_scale).reshape(seq_count, BLK, HEADS, HEAD)
    key_in = (owned[1] * mix_scale).reshape(seq_count, BLK, HEADS, HEAD)
    value = (owned[2] * mix_scale).reshape(seq_count, BLK, HEADS, HEAD)
    gating = (owned[3] * mix_scale).reshape(seq_count, BLK, HEADS, HEAD)
    write_pre = (
        jnp.dot(own_scaled, write_weight, preferred_element_type=jnp.float32) * mix_scale
    ).reshape(seq_count, BLK, HEADS)
    forget_pre = (
        jnp.dot(own_scaled, forget_weight, preferred_element_type=jnp.float32) * mix_scale
    ).reshape(seq_count, BLK, HEADS)
    positions = jnp.arange(BLK, dtype=jnp.int32)
    live = (positions[None, :] < lengths[:, None]).astype(jnp.float32)
    mixed_heads, new_state = delta_block(
        query, key_in, value, gating, write_pre, forget_pre, forget_rate, live, state
    )
    half_cols = mixed_heads.shape[1] // 2
    portion = collect(mixed_heads, ("kv", "tp"), 0)
    first_half = jnp.dot(
        portion[:, :half_cols], out_weight[:half_cols], preferred_element_type=jnp.float32
    ).astype(jnp.bfloat16)
    second_half = jnp.dot(
        portion[:, half_cols:], out_weight[half_cols:], preferred_element_type=jnp.float32
    ).astype(jnp.bfloat16)
    first_half, second_half = lax.optimization_barrier((first_half, second_half))
    mixed_sum = first_half.astype(jnp.float32) + second_half.astype(jnp.float32)
    after_mix = (after_first.astype(jnp.float32) + mixed_sum).astype(jnp.bfloat16)
    mixed_out = feed_forward(after_mix, gain_second, second_gate, second_up, second_down)
    return (mixed_out, new_state)


def solution(mesh):
    in_specs = (
        P("dp", ("kv", "tp")),
        P(("dp", "kv", "tp")),
        P(("dp", "kv", "tp"), None, None, None),
        P(),
        P(None, "kv"),
        P(None, "kv"),
        P("kv", None),
        P(),
        P(None, ("kv", "tp")),
        P(None, ("kv", "tp")),
        P(None, ("kv", "tp")),
        P(None, ("kv", "tp")),
        P(),
        P(),
        P(),
        P(None, ("kv", "tp")),
        P(),
        P(None, "kv"),
        P(None, "kv"),
        P("kv", None),
    )
    out_specs = (P("dp", ("kv", "tp")), P(("dp", "kv", "tp"), None, None, None))
    return jax.shard_map(
        per_device, mesh=mesh, in_specs=in_specs, out_specs=out_specs, check_vma=False
    )
```

profile of v0, /device:TPU:1, one launch (start us, length us, event | category | flops | bytes accessed | tf_op | source)
XLA Modules:
  0.0 314.3 jit_solution(10236440952969772282)
XLA Ops:
  0.6 0.8 copy.214
  1.5 6.6 %all_to_all.103 = bf16[2,256,32]{1,2,0:T(8,128)(2,1)S(1)} all-to-all(bf16[2,256,32]{1,2,0:T(8,128)(2,1)S(1)} %bitcast.179), channel_id=1, replica_groups=mesh['dp'=4,'kv'=32,'tp'=2] {'tp'}, dimensions={0} | all-to-all | bytes 65536 | tf_op jit(solution)/shard_map/all_to_all | solution.py:56
  8.2 35.9 %all_to_all.104 = bf16[32,256,64]{1,2,0:T(8,128)(2,1)S(1)} all-to-all(bf16[32,256,64]{1,2,0:T(8,128)(2,1)S(1)} %broadcast_in_dim.16), channel_id=1, replica_groups=mesh['dp'=4,'kv'=32,'tp'=2] {'kv'}, dimensions={0} | all-to-all | bytes 2097152 | tf_op jit(solution)/shard_map/all_to_all | solution.py:21
  44.0 0.3 multiply_reduce_fusion.1
  44.4 0.3 fusion.1
  44.7 0.4 copy-done.3
  45.1 0.4 convolution_multiply_fusion.3
  45.5 2.3 convolution_convert_fusion.1
  47.8 0.5 copy.146
  48.4 31.3 %all_to_all.105 = bf16[32,256,64]{1,2,0:T(8,128)(2,1)S(1)} all-to-all(bf16[32,256,64]{1,2,0:T(8,128)(2,1)S(1)} %bitcast.167), channel_id=1, replica_groups=mesh['dp'=4,'kv'=32,'tp'=2] {'kv'}, dimensions={0} | all-to-all | bytes 2097152 | tf_op jit(solution)/shard_map/all_to_all | solution.py:35
  79.7 0.2 convert_reduce_fusion.1
  79.8 6.9 %all_to_all.106 = f32[256,2,32]{0,2,1:T(8,128)S(1)} all-to-all(f32[256,2,32]{0,2,1:T(8,128)S(1)} %bitcast.173), channel_id=1, replica_groups=mesh['dp'=4,'kv'=32,'tp'=2] {'tp'}, dimensions={1} | all-to-all | bytes 131072 | tf_op jit(solution)/shard_map/all_to_all | solution.py:60
  86.7 1.6 broadcast_in_dim.17
  88.3 6.2 %all-to-all-start.4 = ((bf16[64,512,32]{1,2,0:T(8,128)(2,1)}), bf16[64,512,32]{1,2,0:T(8,128)(2,1)S(1)}, u32[]{:S(2)}, u32[]{:S(2)}) async-start(bf16[64,512,32]{1,2,0:T(8,128)(2,1)} %broadcast_in_dim.17), calls=%async_computation.4 | async-start | bytes 4194304 | tf_op jit(solution)/shard_map/all_to_all | solution.py:21
  95.3 49.0 %all-to-all-done.4 = bf16[64,512,32]{1,2,0:T(8,128)(2,1)S(1)} async-done(((bf16[64,512,32]{1,2,0:T(8,128)(2,1)}), bf16[64,512,32]{1,2,0:T(8,128)(2,1)S(1)}, u32[]{:S(2)}, u32[]{:S(2)}) %all-to-all-start.4) | async-done | bytes 2097184 | tf_op jit(solution)/shard_map/all_to_all | solution.py:21
  144.3 0.4 multiply_reduce_fusion.2
  144.6 1.0 copy-done.1
  145.6 2.1 multiply_convert_fusion
  147.7 0.5 fusion.14
  148.2 0.4 copy-done.6
  148.6 0.4 fusion.13
  149.1 0.5 fusion.12
  149.6 0.5 fusion.11
  150.1 0.3 copy.148
  150.4 1.1 reshape.443
  151.5 7.0 %all-to-all-start.5 = ((bf16[64,2,512]{2,1,0:T(2,128)(2,1)}), bf16[64,2,512]{2,1,0:T(2,128)(2,1)S(1)}, u32[]{:S(2)}, u32[]{:S(2)}) async-start(bf16[64,2,512]{2,1,0:T(2,128)(2,1)} %reshape.443), calls=%async_computation.5 | async-start | bytes 262144 | tf_op jit(solution)/shard_map/all_to_all | solution.py:149
  158.4 1.4 fusion.63
  160.0 1.3 fusion.68
  161.4 8.1 %all-to-all-done.5 = bf16[64,2,512]{2,1,0:T(2,128)(2,1)S(1)} async-done(((bf16[64,2,512]{2,1,0:T(2,128)(2,1)}), bf16[64,2,512]{2,1,0:T(2,128)(2,1)S(1)}, u32[]{:S(2)}, u32[]{:S(2)}) %all-to-all-start.5) | async-done | bytes 131104 | tf_op jit(solution)/shard_map/all_to_all | solution.py:149
  169.5 0.3 reshape.444
  169.8 0.3 copy.149
  170.1 0.2 copy.150
  170.5 0.1 squeeze.19
  171.0 0.2 fusion.46
  171.5 0.2 fusion.57
  171.7 0.3 fusion.10
  172.0 0.2 fusion.76
  172.2 0.2 fusion.52
  172.5 0.3 convolution_add_fusion.1
  173.0 0.2 fusion.77
  173.3 0.2 fusion.43
  173.5 0.2 convolution_bitcast_fusion.2
  173.8 0.3 convolution_multiply_fusion.4
  174.0 1.0 convolution_bitcast_fusion.3
  175.0 1.0 fusion.9
  176.0 0.3 multiply_reduce_fusion.3
  176.6 0.2 broadcast_in_dim.22
  176.9 53.6 %all_to_all.107 = bf16[64,8,2048]{2,1,0:T(8,128)(2,1)S(1)} all-to-all(bf16[64,8,2048]{2,1,0:T(8,128)(2,1)S(1)} %broadcast_in_dim.22), channel_id=1, replica_groups=mesh['dp'=4,'kv'=32,'tp'=2] {'kv','tp'}, dimensions={0} | all-to-all | bytes 4194304 | tf_op jit(solution)/shard_map/all_to_all | solution.py:21
  230.5 0.4 convolution_convert_fusion.7
  230.9 0.4 convolution_convert_fusion.6
  231.4 5.5 %all_to_all.108 = bf16[2,256,32]{1,2,0:T(8,128)(2,1)S(1)} all-to-all(bf16[2,256,32]{1,2,0:T(8,128)(2,1)S(1)} %bitcast.180), channel_id=1, replica_groups=mesh['dp'=4,'kv'=32,'tp'=2] {'tp'}, dimensions={0} | all-to-all | bytes 65536 | tf_op jit(solution)/shard_map/all_to_all | solution.py:56
  237.0 31.0 %all_to_all.109 = bf16[32,256,64]{1,2,0:T(8,128)(2,1)S(1)} all-to-all(bf16[32,256,64]{1,2,0:T(8,128)(2,1)S(1)} %broadcast_in_dim.23), channel_id=1, replica_groups=mesh['dp'=4,'kv'=32,'tp'=2] {'kv'}, dimensions={0} | all-to-all | bytes 2097152 | tf_op jit(solution)/shard_map/all_to_all | solution.py:21
  268.0 0.3 multiply_reduce_fusion
  268.3 0.3 fusion
  268.6 0.4 copy-done.4
  269.1 0.4 convolution_multiply_fusion.1
  269.4 3.5 %convolution_convert_fusion = bf16[256,2048]{1,0:T(8,128)(2,1)} fusion(bf16[176,2048]{1,0:T(8,128)(2,1)} %param.39, bf16[2048,176]{0,1:T(8,128)(2,1)} %param.38, bf16[256,2048]{0,1:T(8,128)(2,1)S(1)} %fusion, f32[256,176]{0,1:T(8,128)S(1)} %convolution_multiply_fusion.1, f32[256]{0:T(256)S(1)} %add_rsqrt_fusion.3), kind=kOutput, calls=%fused_computation.1 | convolution fusion | flops 369938432 | bytes 3720192 | tf_op jit(solution)/shard_map/dot_general | solution.py:51
  272.9 2.3 copy.175
  275.2 5.9 %all-to-all-start.9 = ((bf16[32,256,64]{1,2,0:T(8,128)(2,1)}), bf16[32,256,64]{1,2,0:T(8,128)(2,1)S(1)}, u32[]{:S(2)}, u32[]{:S(2)}) async-start(bf16[32,256,64]{1,2,0:T(8,128)(2,1)} %bitcast.165), calls=%async_computation.9 | async-start | bytes 2097152 | tf_op jit(solution)/shard_map/all_to_all | solution.py:35
  281.1 2.8 fusion.2
  284.0 22.6 %all-to-all-done.9 = bf16[32,256,64]{1,2,0:T(8,128)(2,1)S(1)} async-done(((bf16[32,256,64]{1,2,0:T(8,128)(2,1)}), bf16[32,256,64]{1,2,0:T(8,128)(2,1)S(1)}, u32[]{:S(2)}, u32[]{:S(2)}) %all-to-all-start.9) | async-done | bytes 1048608 | tf_op jit(solution)/shard_map/all_to_all | solution.py:35
  306.6 0.2 convert_reduce_fusion
  306.8 6.9 %all_to_all.110 = f32[256,2,32]{0,2,1:T(8,128)S(1)} all-to-all(f32[256,2,32]{0,2,1:T(8,128)S(1)} %bitcast.174), channel_id=1, replica_groups=mesh['dp'=4,'kv'=32,'tp'=2] {'tp'}, dimensions={1} | all-to-all | bytes 131072 | tf_op jit(solution)/shard_map/all_to_all | solution.py:60
  313.7 0.6 add_convert_fusion
  (66 shorter events, 1.9 us)
Async XLA Ops:
  0.6 44.9 %copy-start = (bf16[176,2048]{1,0:T(8,128)(2,1)S(1)}, bf16[176,2048]{1,0:T(8,128)(2,1)}, u32[]{:S(2)}) copy-start(bf16[176,2048]{1,0:T(8,128)(2,1)} %param.26) | copy-start | bytes 2162692
  8.1 36.3 %copy-start.10 = (f32[2048]{0:T(1024)S(1)}, f32[2048]{0:T(1024)}, u32[]{:S(2)}) copy-start(f32[2048]{0:T(1024)} %param.23) | copy-start | bytes 24580
  44.0 1.1 copy-start.3
  48.3 38.4 %copy-start.9 = (bf16[512,32]{0,1:T(8,128)(2,1)S(1)}, bf16[512,32]{0,1:T(8,128)(2,1)}, u32[]{:S(2)}) copy-start(bf16[512,32]{0,1:T(8,128)(2,1)} %param.20) | copy-start | bytes 98308
  88.3 6.9 %copy-start.14 = (f32[16]{0:T(128)S(1)}, f32[16]{0:T(128)}, u32[]{:S(2)}) copy-start(f32[16]{0:T(128)} %param.34) | copy-start | bytes 196
  88.3 57.3 %copy-start.11 = (f32[2048]{0:T(1024)S(1)}, f32[2048]{0:T(1024)}, u32[]{:S(2)}) copy-start(f32[2048]{0:T(1024)} %param.27) | copy-start | bytes 24580
  88.3 55.9 %all-to-all-start.4 = ((bf16[64,512,32]{1,2,0:T(8,128)(2,1)}), bf16[64,512,32]{1,2,0:T(8,128)(2,1)S(1)}, u32[]{:S(2)}, u32[]{:S(2)}) async-start(bf16[64,512,32]{1,2,0:T(8,128)(2,1)} %broadcast_in_dim.17), calls=%async_computation.4 | async-start | bytes 4194304 | tf_op jit(solution)/shard_map/all_to_all | solution.py:21
  144.3 1.3 copy-start.1
  145.6 2.1 copy-start.5
  147.7 0.9 copy-start.6
  147.7 1.3 copy-start.7
  148.6 0.9 copy-start.8
  151.5 18.1 %all-to-all-start.5 = ((bf16[64,2,512]{2,1,0:T(2,128)(2,1)}), bf16[64,2,512]{2,1,0:T(2,128)(2,1)S(1)}, u32[]{:S(2)}, u32[]{:S(2)}) async-start(bf16[64,2,512]{2,1,0:T(2,128)(2,1)} %reshape.443), calls=%async_computation.5 | async-start | bytes 262144 | tf_op jit(solution)/shard_map/all_to_all | solution.py:149
  171.0 3.0 copy-start.2
  176.9 53.7 %copy-start.13 = (bf16[2048,32]{0,1:T(8,128)(2,1)S(1)}, bf16[2048,32]{0,1:T(8,128)(2,1)}, u32[]{:S(2)}) copy-start(bf16[2048,32]{0,1:T(8,128)(2,1)} %param.35) | copy-start | bytes 393220
  236.9 31.4 %copy-start.12 = (f32[2048]{0:T(1024)S(1)}, f32[2048]{0:T(1024)}, u32[]{:S(2)}) copy-start(f32[2048]{0:T(1024)} %param.36) | copy-start | bytes 24580
  268.0 1.1 copy-start.4
  275.2 31.4 %all-to-all-start.9 = ((bf16[32,256,64]{1,2,0:T(8,128)(2,1)}), bf16[32,256,64]{1,2,0:T(8,128)(2,1)S(1)}, u32[]{:S(2)}, u32[]{:S(2)}) async-start(bf16[32,256,64]{1,2,0:T(8,128)(2,1)} %bitcast.165), calls=%async_computation.9 | async-start | bytes 2097152 | tf_op jit(solution)/shard_map/all_to_all | solution.py:35
where the time goes:
time: 315 us; the launch traced here: 314 us
  blocking collectives  178 us (57%)
  waiting for transfers between devices  79.8 us (25%)
  starting transfers between devices  19.1 us (6%)
  matrix products  19 us (6%)
  local copies, waits for them, and re-layouts  11.6 us (4%)
  other arithmetic  5.37 us (2%)
    all_to_all x3, blocking collectives, copy_for_each(): return lax.all_to_all(copies, axis, split_axis=0, concat_axis=0, tiled=True)  120 us
    all_to_all x1, waiting for transfers between devices, copy_for_each(): return lax.all_to_all(copies, axis, split_axis=0, concat_axis=0, tiled=True)  49 us
    all_to_all x1, blocking collectives, sum_at_owner(): lax.all_to_all(parts, axis, split_axis=0, concat_axis=0, tiled=True)  31.3 us
    all_to_all x1, waiting for transfers between devices, sum_at_owner(): lax.all_to_all(parts, axis, split_axis=0, concat_axis=0, tiled=True)  22.6 us
    all_to_all x2, blocking collectives, feed_forward(): lax.all_to_all(partial_value, 'tp', split_axis=1, concat_axis=0, tiled=True)  13.8 us
    all_to_all x2, blocking collectives, feed_forward(): lax.all_to_all(hidden_in, 'tp', split_axis=0, concat_axis=1, tiled=True)  12.1 us
    all_to_all x1, waiting for transfers between devices, per_device(): lax.all_to_all(stacked.astype(jnp.bfloat16), ('kv', 'tp'), split_axis=1,...  8.14 us
    all_to_all x1, starting transfers between devices, per_device(): lax.all_to_all(stacked.astype(jnp.bfloat16), ('kv', 'tp'), split_axis=1,...  6.97 us
  transfers between devices with their start and end apart: 3, of which 3 were waited for; matrix products, arithmetic and copies ran while one was open for 2% of the time, Pallas kernels for 0%

commit v1 on v0

--- a/solution.py
+++ b/solution.py
@@ -146,8 +146,14 @@
             for matrix in (query_weight, key_weight, value_weight, gating_weight)
         ]
     )
-    owned = lax.all_to_all(
-        stacked.astype(jnp.bfloat16), ("kv", "tp"), split_axis=1, concat_axis=2, tiled=True
+    owned = jnp.concatenate(
+        lax.all_to_all(
+            jnp.stack(jnp.split(stacked.astype(jnp.bfloat16), lax.axis_size(("kv", "tp")), axis=1)),
+            ("kv", "tp"),
+            0,
+            0,
+        ),
+        axis=2,
     ).astype(stacked.dtype)
     row_start = lax.axis_index(("kv", "tp")) * own_count
     own_values = lax.dynamic_slice_in_dim(whole_rows, row_start, own_count, 0).astype(jnp.float32)

time: 315 us -> 360 us (1.14)
  local copies, waits for them, and re-layouts: 11.6 us -> 56.3 us
    unnamed x32 -> x99, local copies, waits for them, and re-layouts: 3.71 us -> 46.5 us
  transfers between devices with their start and end apart: 3 -> 3, of which waited for: 3 -> 3; matrix products, arithmetic and copies ran while one was open for 2% -> 1% of each run, Pallas kernels for 0% -> 0%
where the time goes in v1:
time: 360 us; the launch traced here: 359 us
  blocking collectives  178 us (49%)
  waiting for transfers between devices  81.4 us (23%)
  local copies, waits for them, and re-layouts  56.3 us (16%)
  starting transfers between devices  19.1 us (5%)
  matrix products  17.3 us (5%)
  other arithmetic  5.5 us (2%)
    all_to_all x3, blocking collectives, copy_for_each(): return lax.all_to_all(copies, axis, split_axis=0, concat_axis=0, tiled=True)  120 us
    all_to_all x1, waiting for transfers between devices, copy_for_each(): return lax.all_to_all(copies, axis, split_axis=0, concat_axis=0, tiled=True)  49 us
    unnamed x99, local copies, waits for them, and re-layouts  46.5 us
    all_to_all x1, blocking collectives, sum_at_owner(): lax.all_to_all(parts, axis, split_axis=0, concat_axis=0, tiled=True)  31.3 us
    all_to_all x1, waiting for transfers between devices, sum_at_owner(): lax.all_to_all(parts, axis, split_axis=0, concat_axis=0, tiled=True)  22.7 us
    all_to_all x2, blocking collectives, feed_forward(): lax.all_to_all(partial_value, 'tp', split_axis=1, concat_axis=0, tiled=True)  13.8 us
    all_to_all x2, blocking collectives, feed_forward(): lax.all_to_all(hidden_in, 'tp', split_axis=0, concat_axis=1, tiled=True)  12.1 us
    all_to_all x1, waiting for transfers between devices, per_device(): lax.all_to_all(jnp.stack(jnp.split(stacked.astype(jnp.bfloat16), lax.axis...  9.8 us
  transfers between devices with their start and end apart: 3, of which 3 were waited for; matrix products, arithmetic and copies ran while one was open for 1% of the time, Pallas kernels for 0%

profile of v1, /device:TPU:1, one launch (start us, length us, event | category | flops | bytes accessed | tf_op | source)
XLA Modules:
  0.0 359.2 jit_solution(646325436817868259)
XLA Ops:
  0.6 0.8 copy.368
  1.5 6.6 %all_to_all.99 = bf16[2,256,32]{1,2,0:T(8,128)(2,1)S(1)} all-to-all(bf16[2,256,32]{1,2,0:T(8,128)(2,1)S(1)} %bitcast.429), channel_id=1, replica_groups=mesh['dp'=4,'kv'=32,'tp'=2] {'tp'}, dimensions={0} | all-to-all | bytes 65536 | tf_op jit(solution)/shard_map/all_to_all | solution.py:56
  8.2 35.9 %all_to_all.100 = bf16[32,256,64]{1,2,0:T(8,128)(2,1)S(1)} all-to-all(bf16[32,256,64]{1,2,0:T(8,128)(2,1)S(1)} %broadcast_in_dim.16), channel_id=1, replica_groups=mesh['dp'=4,'kv'=32,'tp'=2] {'kv'}, dimensions={0} | all-to-all | bytes 2097152 | tf_op jit(solution)/shard_map/all_to_all | solution.py:21
  45.5 2.3 convolution_convert_fusion.1
  48.4 31.3 %all_to_all.101 = bf16[32,256,64]{1,2,0:T(8,128)(2,1)S(1)} all-to-all(bf16[32,256,64]{1,2,0:T(8,128)(2,1)S(1)} %bitcast.419), channel_id=1, replica_groups=mesh['dp'=4,'kv'=32,'tp'=2] {'kv'}, dimensions={0} | all-to-all | bytes 2097152 | tf_op jit(solution)/shard_map/all_to_all | solution.py:35
  79.8 6.9 %all_to_all.102 = f32[256,2,32]{0,2,1:T(8,128)S(1)} all-to-all(f32[256,2,32]{0,2,1:T(8,128)S(1)} %bitcast.423), channel_id=1, replica_groups=mesh['dp'=4,'kv'=32,'tp'=2] {'tp'}, dimensions={1} | all-to-all | bytes 131072 | tf_op jit(solution)/shard_map/all_to_all | solution.py:60
  86.7 1.6 broadcast_in_dim.17
  88.3 6.2 %all-to-all-start.4 = ((bf16[64,512,32]{1,2,0:T(8,128)(2,1)}), bf16[64,512,32]{1,2,0:T(8,128)(2,1)S(1)}, u32[]{:S(2)}, u32[]{:S(2)}) async-start(bf16[64,512,32]{1,2,0:T(8,128)(2,1)} %broadcast_in_dim.17), calls=%async_computation.4 | async-start | bytes 4194304 | tf_op jit(solution)/shard_map/all_to_all | solution.py:21
  95.3 49.0 %all-to-all-done.4 = bf16[64,512,32]{1,2,0:T(8,128)(2,1)S(1)} async-done(((bf16[64,512,32]{1,2,0:T(8,128)(2,1)}), bf16[64,512,32]{1,2,0:T(8,128)(2,1)S(1)}, u32[]{:S(2)}, u32[]{:S(2)}) %all-to-all-start.4) | async-done | bytes 2097184 | tf_op jit(solution)/shard_map/all_to_all | solution.py:21
  144.6 1.0 copy-done.1
  145.6 2.1 multiply_convert_fusion
  150.6 0.7 constant_dynamic-update-slice_fusion.62
  152.0 0.7 constant_dynamic-update-slice_fusion.60
  153.4 0.7 constant_dynamic-update-slice_fusion.58
  154.8 0.7 constant_dynamic-update-slice_fusion.56
  155.4 0.7 constant_dynamic-update-slice_fusion.55
  156.1 0.7 constant_dynamic-update-slice_fusion.54
  156.8 0.7 constant_dynamic-update-slice_fusion.53
  157.5 0.7 constant_dynamic-update-slice_fusion.52
  158.2 0.7 constant_dynamic-update-slice_fusion.51
  159.6 0.7 constant_dynamic-update-slice_fusion.49
  160.2 0.7 constant_dynamic-update-slice_fusion.48
  161.5 0.7 constant_dynamic-update-slice_fusion.46
  162.9 0.7 constant_dynamic-update-slice_fusion.44
  167.0 0.7 constant_dynamic-update-slice_fusion.38
  167.7 0.7 constant_dynamic-update-slice_fusion.37
  168.4 0.7 constant_dynamic-update-slice_fusion.36
  169.1 0.7 constant_dynamic-update-slice_fusion.35
  169.8 0.7 constant_dynamic-update-slice_fusion.34
  171.1 0.7 constant_dynamic-update-slice_fusion.32
  172.4 0.7 constant_dynamic-update-slice_fusion.30
  173.8 0.7 constant_dynamic-update-slice_fusion.28
  175.2 0.7 constant_dynamic-update-slice_fusion.26
  176.5 0.7 constant_dynamic-update-slice_fusion.24
  177.9 0.7 constant_dynamic-update-slice_fusion.22
  179.3 0.7 constant_dynamic-update-slice_fusion.20
  180.7 0.7 constant_dynamic-update-slice_fusion.18
  183.3 0.7 constant_dynamic-update-slice_fusion.14
  184.0 0.7 constant_dynamic-update-slice_fusion.13
  184.7 0.7 constant_dynamic-update-slice_fusion.12
  185.4 0.7 constant_dynamic-update-slice_fusion.11
  186.0 0.7 constant_dynamic-update-slice_fusion.10
  187.4 0.7 constant_dynamic-update-slice_fusion.8
  188.8 0.7 constant_dynamic-update-slice_fusion.6
  189.5 0.7 constant_dynamic-update-slice_fusion.5
  190.2 0.7 constant_dynamic-update-slice_fusion.4
  190.8 0.7 constant_dynamic-update-slice_fusion.3
  191.5 0.7 constant_dynamic-update-slice_fusion.2
  192.9 0.7 constant_dynamic-update-slice_fusion
  193.6 2.0 copy.304
  195.6 1.1 reshape.442
  196.7 7.0 %all-to-all-start.5 = ((bf16[64,2,512]{2,1,0:T(2,128)(2,1)}), bf16[64,2,512]{2,1,0:T(2,128)(2,1)S(1)}, u32[]{:S(2)}, u32[]{:S(2)}) async-start(bf16[64,2,512]{2,1,0:T(2,128)(2,1)} %reshape.442), calls=%async_computation.5 | async-start | bytes 262144 | tf_op jit(solution)/shard_map/all_to_all | solution.py:150
  204.9 9.8 %all-to-all-done.5 = bf16[64,2,512]{2,1,0:T(2,128)(2,1)S(1)} async-done(((bf16[64,2,512]{2,1,0:T(2,128)(2,1)}), bf16[64,2,512]{2,1,0:T(2,128)(2,1)S(1)}, u32[]{:S(2)}, u32[]{:S(2)}) %all-to-all-start.5) | async-done | bytes 131104 | tf_op jit(solution)/shard_map/all_to_all | solution.py:150
  218.7 1.0 convolution_bitcast_fusion.3
  219.7 1.0 fusion.9
  221.7 53.6 %all_to_all.103 = bf16[64,8,2048]{2,1,0:T(8,128)(2,1)S(1)} all-to-all(bf16[64,8,2048]{2,1,0:T(8,128)(2,1)S(1)} %broadcast_in_dim.22), channel_id=1, replica_groups=mesh['dp'=4,'kv'=32,'tp'=2] {'kv','tp'}, dimensions={0} | all-to-all | bytes 4194304 | tf_op jit(solution)/shard_map/all_to_all | solution.py:21
  276.2 5.5 %all_to_all.104 = bf16[2,256,32]{1,2,0:T(8,128)(2,1)S(1)} all-to-all(bf16[2,256,32]{1,2,0:T(8,128)(2,1)S(1)} %bitcast.430), channel_id=1, replica_groups=mesh['dp'=4,'kv'=32,'tp'=2] {'tp'}, dimensions={0} | all-to-all | bytes 65536 | tf_op jit(solution)/shard_map/all_to_all | solution.py:56
  281.8 31.0 %all_to_all.105 = bf16[32,256,64]{1,2,0:T(8,128)(2,1)S(1)} all-to-all(bf16[32,256,64]{1,2,0:T(8,128)(2,1)S(1)} %broadcast_in_dim.23), channel_id=1, replica_groups=mesh['dp'=4,'kv'=32,'tp'=2] {'kv'}, dimensions={0} | all-to-all | bytes 2097152 | tf_op jit(solution)/shard_map/all_to_all | solution.py:21
  314.3 3.5 convolution_convert_fusion
  317.7 2.2 copy.329
  320.0 5.9 %all-to-all-start.9 = ((bf16[32,256,64]{1,2,0:T(8,128)(2,1)}), bf16[32,256,64]{1,2,0:T(8,128)(2,1)S(1)}, u32[]{:S(2)}, u32[]{:S(2)}) async-start(bf16[32,256,64]{1,2,0:T(8,128)(2,1)} %bitcast.418), calls=%async_computation.9 | async-start | bytes 2097152 | tf_op jit(solution)/shard_map/all_to_all | solution.py:35
  325.9 2.8 fusion.2
  328.8 22.7 %all-to-all-done.9 = bf16[32,256,64]{1,2,0:T(8,128)(2,1)S(1)} async-done(((bf16[32,256,64]{1,2,0:T(8,128)(2,1)}), bf16[32,256,64]{1,2,0:T(8,128)(2,1)S(1)}, u32[]{:S(2)}, u32[]{:S(2)}) %all-to-all-start.9) | async-done | bytes 1048608 | tf_op jit(solution)/shard_map/all_to_all | solution.py:35
  351.6 6.9 %all_to_all.106 = f32[256,2,32]{0,2,1:T(8,128)S(1)} all-to-all(f32[256,2,32]{0,2,1:T(8,128)S(1)} %bitcast.424), channel_id=1, replica_groups=mesh['dp'=4,'kv'=32,'tp'=2] {'tp'}, dimensions={1} | all-to-all | bytes 131072 | tf_op jit(solution)/shard_map/all_to_all | solution.py:60
  (133 shorter events, 31.6 us)
Async XLA Ops:
  0.6 44.9 %copy-start = (bf16[176,2048]{1,0:T(8,128)(2,1)S(1)}, bf16[176,2048]{1,0:T(8,128)(2,1)}, u32[]{:S(2)}) copy-start(bf16[176,2048]{1,0:T(8,128)(2,1)} %param.26) | copy-start | bytes 2162692
  8.1 36.3 %copy-start.12 = (f32[2048]{0:T(1024)S(1)}, f32[2048]{0:T(1024)}, u32[]{:S(2)}) copy-start(f32[2048]{0:T(1024)} %param.23) | copy-start | bytes 24580
  44.0 1.1 copy-start.3
  48.3 38.4 %copy-start.9 = (bf16[512,32]{0,1:T(8,128)(2,1)S(1)}, bf16[512,32]{0,1:T(8,128)(2,1)}, u32[]{:S(2)}) copy-start(bf16[512,32]{0,1:T(8,128)(2,1)} %param.20) | copy-start | bytes 98308
  88.3 6.9 %copy-start.16 = (f32[16]{0:T(128)S(1)}, f32[16]{0:T(128)}, u32[]{:S(2)}) copy-start(f32[16]{0:T(128)} %param.34) | copy-start | bytes 196
  88.3 57.3 %copy-start.13 = (f32[2048]{0:T(1024)S(1)}, f32[2048]{0:T(1024)}, u32[]{:S(2)}) copy-start(f32[2048]{0:T(1024)} %param.27) | copy-start | bytes 24580
  88.3 55.9 %all-to-all-start.4 = ((bf16[64,512,32]{1,2,0:T(8,128)(2,1)}), bf16[64,512,32]{1,2,0:T(8,128)(2,1)S(1)}, u32[]{:S(2)}, u32[]{:S(2)}) async-start(bf16[64,512,32]{1,2,0:T(8,128)(2,1)} %broadcast_in_dim.17), calls=%async_computation.4 | async-start | bytes 4194304 | tf_op jit(solution)/shard_map/all_to_all | solution.py:21
  144.3 1.3 copy-start.1
  145.6 2.1 copy-start.5
  147.7 0.9 copy-start.6
  147.7 1.3 copy-start.7
  148.6 0.9 copy-start.8
  186.7 16.9 %copy-start.10 = (bf16[2048,16]{0,1:T(8,128)(2,1)S(1)}, bf16[2048,16]{0,1:T(8,128)(2,1)}, u32[]{:S(2)}) copy-start(bf16[2048,16]{0,1:T(8,128)(2,1)} %param.33) | copy-start | bytes 196612
  192.9 11.4 %copy-start.11 = (bf16[2048,16]{0,1:T(8,128)(2,1)S(1)}, bf16[2048,16]{0,1:T(8,128)(2,1)}, u32[]{:S(2)}) copy-start(bf16[2048,16]{0,1:T(8,128)(2,1)} %param.32) | copy-start | bytes 196612
  196.7 18.1 %all-to-all-start.5 = ((bf16[64,2,512]{2,1,0:T(2,128)(2,1)}), bf16[64,2,512]{2,1,0:T(2,128)(2,1)S(1)}, u32[]{:S(2)}, u32[]{:S(2)}) async-start(bf16[64,2,512]{2,1,0:T(2,128)(2,1)} %reshape.442), calls=%async_computation.5 | async-start | bytes 262144 | tf_op jit(solution)/shard_map/all_to_all | solution.py:150
  215.6 3.1 copy-start.2
  221.7 53.7 %copy-start.15 = (bf16[2048,32]{0,1:T(8,128)(2,1)S(1)}, bf16[2048,32]{0,1:T(8,128)(2,1)}, u32[]{:S(2)}) copy-start(bf16[2048,32]{0,1:T(8,128)(2,1)} %param.35) | copy-start | bytes 393220
  281.7 31.4 %copy-start.14 = (f32[2048]{0:T(1024)S(1)}, f32[2048]{0:T(1024)}, u32[]{:S(2)}) copy-start(f32[2048]{0:T(1024)} %param.36) | copy-start | bytes 24580
  312.8 1.1 copy-start.4
  320.0 31.4 %all-to-all-start.9 = ((bf16[32,256,64]{1,2,0:T(8,128)(2,1)}), bf16[32,256,64]{1,2,0:T(8,128)(2,1)S(1)}, u32[]{:S(2)}, u32[]{:S(2)}) async-start(bf16[32,256,64]{1,2,0:T(8,128)(2,1)} %bitcast.418), calls=%async_computation.9 | async-start | bytes 2097152 | tf_op jit(solution)/shard_map/all_to_all | solution.py:35
